TPU v7x, 32 devices: a whole 2x2x4 slice. The times are simulated.
32 devices in a mesh: ep: 16 (over z, y, x), tp: 2 (over core).
Axes of the slice: x: 2, y: 2, z: 4, core: 2. Of those that a mesh axis runs over, the one named last changes fastest.
Arguments:
- tokens: bfloat16 [512, 3072], P('ep'), may hold values from -6 to 6
- carried: float32 [512, 96, 128], P('ep', 'tp'), may hold values from -4 to 4
- decay_rate: float32 [96, 64], P('tp'), may hold values from 0.02 to 20
- frequency: float32 [96, 64], P('tp'), may hold values from 0 to 200
- log_step: float32 [96], P('tp'), may hold values from -4.6 to 0
- in_map: bfloat16 [96, 128, 16], P('tp'), may hold values from -1 to 1
- out_map: bfloat16 [96, 16, 128], P('tp'), may hold values from -0.5 to 0.5
- skip_gain: float32 [1536], P('tp'), may hold values from -4 to 4
- norm_gain: float32 [3072], replicated, may hold values from 0.1 to 1.9
- w_in: bfloat16 [3072, 1536], P(None, 'tp'), may hold values from -0.109375 to 0.109375
- w_out: bfloat16 [1536, 3072], P('tp'), may hold values from -0.15625 to 0.15625
- expert_gain: float32 [3072], replicated, may hold values from 0.1 to 1.9
- route_ids: int32 [512, 2], P('ep'), may hold values from 0 to 7, all different within a row; in each aligned block of 32 rows (0 to 31, 32 to 63, ...) at most 16 rows name the same one
- route_logit: float32 [512, 2], P('ep'), may hold values from -6 to 6
- w_gate: bfloat16 [3072, 43008], P(None, ('ep', 'tp')), may hold values from -0.109375 to 0.109375
- w_up: bfloat16 [3072, 43008], P(None, ('ep', 'tp')), may hold values from -0.109375 to 0.109375
- w_down: bfloat16 [43008, 3072], P(('ep', 'tp')), may hold values from -0.078125 to 0.078125
Outputs:
- new_tokens: bfloat16 [512, 3072], P('ep', 'tp')
- new_carried: float32 [512, 96, 128], P('ep', 'tp')
Inputs may be any that keep to these rules, and one draw needn't show every extreme that they name: `route_ids`: each row names 2 different experts; within each aligned block of 32 rows (the rows of one index of ep) no expert is named by more than 16 rows, a bound that some block reaches.
All inputs are finite; a program needn't handle non-finite values.
Results may differ from a plain program's by a relative error of at most 0.014.
Values may be sent and summed in bfloat16 or wider, within the bound.
A program may use at most 128 MiB of HBM per device.

v0:
```python
import jax
import jax.numpy as jnp
from jax import lax
from jax.sharding import PartitionSpec as P

EXPERTS = 8
TOP = 2
CAP = 16


def normalize(rows, gain):
    wide = rows.astype(jnp.float32)
    scaled = wide * lax.rsqrt(jnp.mean(wide * wide, axis=-1, keepdims=True) + 1e-06)
    return (scaled * gain).astype(jnp.bfloat16)


def state_update(drive, carried, decay_rate, frequency, log_step, in_map, out_map, skip_gain):
    count_rows, width = drive.shape
    groups, half = decay_rate.shape
    channels = width // groups
    step_size = jnp.exp(log_step)[:, None]
    magnitude = jnp.exp(-decay_rate * step_size)
    real_decay = magnitude * jnp.cos(frequency * step_size)
    imag_decay = magnitude * jnp.sin(frequency * step_size)
    denom = decay_rate * decay_rate + frequency * frequency
    real_less = real_decay - 1.0
    real_factor = (-real_less * decay_rate + imag_decay * frequency) / denom
    imag_factor = (-imag_decay * decay_rate - real_less * frequency) / denom
    grouped_drive = drive.reshape(count_rows, groups, channels)
    projected = jnp.einsum(
        "sgh,gqh->sgq", grouped_drive, in_map, preferred_element_type=jnp.float32
    )
    real_in = projected[..., :half]
    imag_in = projected[..., half:]
    real_push = real_factor * real_in - imag_factor * imag_in
    imag_push = real_factor * imag_in + imag_factor * real_in
    real_old = carried[..., :half]
    imag_old = carried[..., half:]
    real_new = real_decay * real_old - imag_decay * imag_old + real_push
    imag_new = real_decay * imag_old + imag_decay * real_old + imag_push
    joined = jnp.concatenate([real_new, -imag_new], axis=-1)
    reading = jnp.einsum(
        "sgq,ghq->sgh", joined, out_map.astype(jnp.float32), precision=lax.Precision.HIGHEST
    )
    total = reading.reshape(count_rows, width) + skip_gain * drive.astype(jnp.float32)
    activated = jax.nn.gelu(total).astype(jnp.bfloat16)
    return (activated, jnp.concatenate([real_new, imag_new], axis=-1))


def route_weights(route_logit):
    first = jax.nn.sigmoid(route_logit[:, 0] - route_logit[:, 1])
    second = jax.nn.sigmoid(route_logit[:, 1] - route_logit[:, 0])
    return jnp.stack([first, second], axis=1)


def per_device(
    tokens,
    carried,
    decay_rate,
    frequency,
    log_step,
    in_map,
    out_map,
    skip_gain,
    norm_gain,
    w_in,
    w_out,
    expert_gain,
    route_ids,
    route_logit,
    w_gate,
    w_up,
    w_down,
):
    count_rows, model_width = tokens.shape
    normed = normalize(tokens, norm_gain)
    drive = jnp.dot(normed, w_in, preferred_element_type=jnp.float32).astype(jnp.bfloat16)
    activated, new_carried = state_update(
        drive, carried, decay_rate, frequency, log_step, in_map, out_map, skip_gain
    )
    partial_value = jnp.dot(activated, w_out, preferred_element_type=jnp.float32).astype(
        jnp.bfloat16
    )
    summed = lax.psum(partial_value.astype(jnp.float32).astype(jnp.bfloat16), "tp").astype(
        jnp.float32
    )
    mixed = (tokens.astype(jnp.float32) + summed).astype(jnp.bfloat16)
    expert_in = normalize(mixed, expert_gain)
    weights = route_weights(route_logit)
    ep_count = lax.axis_size("ep")
    group_size = ep_count // EXPERTS
    expert_ids = jnp.arange(EXPERTS, dtype=jnp.int32)
    routes_flat = route_ids.reshape(-1)
    weights_flat = weights.reshape(-1)
    onehot = (routes_flat[:, None] == expert_ids[None, :]).astype(jnp.int32)
    earlier = jnp.cumsum(onehot, axis=0) - onehot
    slot_index = jnp.sum(earlier * onehot, axis=1)
    position = routes_flat * CAP + slot_index
    placement = (jnp.arange(EXPERTS * CAP, dtype=jnp.int32)[:, None] == position[None, :]).astype(
        jnp.float32
    )
    per_token = placement.reshape(EXPERTS * CAP, count_rows, TOP).sum(axis=2)
    packed = jnp.dot(per_token.astype(jnp.bfloat16), expert_in, preferred_element_type=jnp.float32)
    packed = packed.astype(jnp.bfloat16).reshape(EXPERTS, CAP, model_width)
    outgoing = jnp.repeat(packed, group_size, axis=0)
    received = lax.all_to_all(outgoing, "ep", split_axis=0, concat_axis=0, tiled=True)
    sources, slots, features = received.shape
    rows = received.reshape(sources * slots, features)
    gated = jnp.dot(rows, w_gate, preferred_element_type=jnp.float32)
    upward = jnp.dot(rows, w_up, preferred_element_type=jnp.float32)
    hidden = (jax.nn.silu(gated) * upward).astype(jnp.bfloat16)
    produced = jnp.dot(hidden, w_down, preferred_element_type=jnp.float32)
    produced = produced.reshape(sources, slots, features)
    halves = lax.psum_scatter(
        produced.astype(jnp.bfloat16), "tp", scatter_dimension=2, tiled=True
    ).astype(jnp.float32)
    returned = lax.all_to_all(
        halves.astype(jnp.bfloat16), "ep", split_axis=0, concat_axis=0, tiled=True
    ).astype(halves.dtype)
    per_expert = returned.reshape(EXPERTS, group_size, CAP, -1).sum(axis=1)
    per_expert = per_expert.reshape(EXPERTS * CAP, -1)
    weighing = (
        (placement * weights_flat[None, :]).reshape(EXPERTS * CAP, count_rows, TOP).sum(axis=2)
    )
    expert_sum = jnp.dot(
        weighing.T, per_expert, preferred_element_type=jnp.float32, precision=lax.Precision.HIGHEST
    )
    half_width = model_width // lax.axis_size("tp")
    column_start = lax.axis_index("tp") * half_width
    own_mixed = lax.dynamic_slice_in_dim(mixed, column_start, half_width, 1)
    new_tokens = (own_mixed.astype(jnp.float32) + expert_sum).astype(jnp.bfloat16)
    return (new_tokens, new_carried)


def solution(mesh):
    return jax.shard_map(
        per_device,
        mesh=mesh,
        in_specs=(
            P("ep", None),
            P("ep", "tp", None),
            P("tp", None),
            P("tp", None),
            P("tp"),
            P("tp", None, None),
            P("tp", None, None),
            P("tp"),
            P(),
            P(None, "tp"),
            P("tp", None),
            P(),
            P("ep", None),
            P("ep", None),
            P(None, ("ep", "tp")),
            P(None, ("ep", "tp")),
            P(("ep", "tp"), None),
        ),
        out_specs=(P("ep", "tp"), P("ep", "tp", None)),
        check_vma=False,
    )
```

profile of v0, /device:TPU:0, one launch (start us, length us, event | category | flops | bytes accessed | tf_op | source)
XLA Modules:
  0.0 152.5 jit_solution(15072366406423989595)
XLA Ops:
  7.2 0.7 exp.18
  7.9 1.1 fusion.9
  9.0 3.5 %convolution_convert_fusion.3 = bf16[32,768]{1,0:T(8,128)(2,1)S(1)} fusion(bf16[3072,768]{1,0:T(8,128)(2,1)} %param.26, bf16[32,3072]{1,0:T(8,128)(2,1)} %param.17, f32[3072]{0:T(1024)} %param.25, f32[32]{0:T(128)S(1)} %add_rsqrt_fusion.1), kind=kOutput, calls=%fused_computation.9 | convolution fusion | flops 151412736 | bytes 4976768 | tf_op jit(solution)/shard_map/dot_general | solution.py:77
  12.5 0.2 copy.48
  12.7 0.3 fusion.44
  13.0 0.3 convolution_bitcast_fusion
  13.4 0.2 cosine_multiply_fusion
  13.6 0.8 fusion.43
  14.6 0.8 fusion.2
  15.6 4.0 %convolution_convert_fusion.2 = bf16[32,3072]{1,0:T(8,128)(2,1)} fusion(bf16[768,3072]{1,0:T(8,128)(2,1)} %param.27, f32[32,768]{1,0:T(8,128)S(1)} %copy.49, bf16[32,768]{1,0:T(8,128)(2,1)S(1)} %convolution_convert_fusion.3, f32[768]{0:T(1024)S(1)} %copy-done.8), kind=kOutput, calls=%fused_computation.2 | convolution fusion | flops 151388160 | bytes 5065728 | tf_op jit(solution)/shard_map/dot_general | solution.py:81
  20.0 0.2 select_reduce_fusion.1
  20.5 20.0 %all-reduce.2.cloned.1.call-done = bf16[32,3072]{1,0:T(8,128)(2,1)} async-done(((bf16[32,3072]{1,0:T(8,128)(2,1)}), bf16[32,3072]{1,0:T(8,128)(2,1)}) %all-reduce.2.cloned.1.call-update) | async-done | bytes 196624 | tf_op jit(solution)/shard_map/psum | solution.py:84
  40.5 1.1 fusion.6
  41.6 0.4 convolution_convert_fusion.1
  42.1 0.2 broadcast_in_dim.2
  42.3 44.6 %all_to_all.10 = bf16[16,16,3072]{2,1,0:T(8,128)(2,1)S(1)} all-to-all(bf16[16,16,3072]{2,1,0:T(8,128)(2,1)S(1)} %bitcast.27), channel_id=1, replica_groups=mesh['ep'=16,'tp'=2] {'ep'}, dimensions={0} | all-to-all | bytes 3145728 | tf_op jit(solution)/shard_map/all_to_all | solution.py:106
  86.9 6.8 %fusion.45 = f32[256,1344]{0,1:T(8,128)} fusion(bf16[256,3072]{1,0:T(8,128)(2,1)S(1)} %bitcast.31, bf16[3072,1344]{0,1:T(8,128)(2,1)} %param.31), kind=kOutput, calls=%fused_computation.74 | convolution fusion | flops 2113929216 | bytes 11206656 | tf_op jit(solution)/shard_map/dot_general | solution.py:109
  93.6 16.3 %convolution_convert_fusion = bf16[256,3072]{1,0:T(8,128)(2,1)} fusion(bf16[1344,3072]{1,0:T(8,128)(2,1)} %param.33, bf16[256,3072]{1,0:T(8,128)(2,1)S(1)} %bitcast.32, bf16[3072,1344]{0,1:T(8,128)(2,1)} %param.32, f32[256,1344]{0,1:T(8,128)} %fusion.45), kind=kOutput, calls=%fused_computation | convolution fusion | flops 4230709248 | bytes 21037056 | tf_op jit(solution)/shard_map/dot_general | solution.py:112
  110.0 7.5 %reduce-scatter.2.cloned.1.call-done = bf16[16,16,1536]{2,1,0:T(8,128)(2,1)} async-done(((bf16[16,16,3072]{2,1,0:T(8,128)(2,1)}), bf16[16,16,1536]{2,1,0:T(8,128)(2,1)}) %reduce-scatter.2.cloned.1.call-update) | async-done | bytes 786448 | tf_op jit(solution)/shard_map/reduce_scatter | solution.py:114
  117.4 6.9 %all-to-all-start.1 = ((bf16[16,16,1536]{2,1,0:T(8,128)(2,1)}), bf16[16,16,1536]{2,1,0:T(8,128)(2,1)S(1)}, u32[]{:S(2)}, u32[]{:S(2)}) async-start(bf16[16,16,1536]{2,1,0:T(8,128)(2,1)} %reduce-scatter.2.cloned.1.call-done), calls=%async_computation.2 | async-start | bytes 1572864 | tf_op jit(solution)/shard_map/all_to_all | solution.py:117
  124.3 0.3 pad_maximum_fusion
  124.6 1.3 copy.52
  126.0 18.4 %all-to-all-done.1 = bf16[16,16,1536]{2,1,0:T(8,128)(2,1)S(1)} async-done(((bf16[16,16,1536]{2,1,0:T(8,128)(2,1)}), bf16[16,16,1536]{2,1,0:T(8,128)(2,1)S(1)}, u32[]{:S(2)}, u32[]{:S(2)}) %all-to-all-start.1) | async-done | bytes 786464 | tf_op jit(solution)/shard_map/all_to_all | solution.py:117
  144.5 1.2 fusion.1
  (38 shorter events, 1.4 us)
Async XLA Ops:
  7.2 5.8 %copy-start = (bf16[48,128,16]{1,2,0:T(8,128)(2,1)S(1)}, bf16[48,128,16]{1,2,0:T(8,128)(2,1)}, u32[]{:S(2)}) copy-start(bf16[48,128,16]{1,2,0:T(8,128)(2,1)} %param.22) | copy-start | bytes 589828
  7.2 33.3 %all-reduce.2.cloned.1.call-start = ((), (), s32[]{:S(2)}) async-start(), calls=%async_computation.3 | async-start | bytes 393216 | tf_op jit(solution)/shard_map/psum | solution.py:84
  9.0 3.7 %copy-start.1 = (f32[32,48,128]{2,1,0:T(8,128)S(1)}, f32[32,48,128]{2,1,0:T(8,128)}, u32[]{:S(2)}) copy-start(f32[32,48,128]{2,1,0:T(8,128)} %param.18) | copy-start | bytes 2359300
  12.7 0.7 copy-start.4
  12.7 0.7 copy-start.5
  13.6 0.9 copy-start.3
  14.4 1.1 copy-start.8
  15.5 4.1 %copy-start.9 = (f32[32,2]{0,1:T(2,128)S(1)}, f32[32,2]{0,1:T(2,128)}, u32[]{:S(2)}) copy-start(f32[32,2]{0,1:T(2,128)} %param.30) | copy-start | bytes 772
  15.6 4.1 %copy-start.7 = (s32[32,2]{0,1:T(2,128)S(1)}, s32[32,2]{0,1:T(2,128)}, u32[]{:S(2)}) copy-start(s32[32,2]{0,1:T(2,128)} %param.29) | copy-start | bytes 772
  15.6 25.0 %copy-start.2 = (bf16[32,3072]{1,0:T(8,128)(2,1)S(1)}, bf16[32,3072]{1,0:T(8,128)(2,1)}, u32[]{:S(2)}) copy-start(bf16[32,3072]{1,0:T(8,128)(2,1)} %param.17) | copy-start | bytes 589828
  15.6 26.1 %copy-start.6 = (f32[3072]{0:T(1024)S(1)}, f32[3072]{0:T(1024)}, u32[]{:S(2)}) copy-start(f32[3072]{0:T(1024)} %param.28) | copy-start | bytes 36868
  19.6 97.9 %reduce-scatter.2.cloned.1.call-start = ((), (), s32[]{:S(2)}) async-start(), calls=%async_computation.4 | async-start | bytes 2359296 | tf_op jit(solution)/shard_map/reduce_scatter | solution.py:114
  117.4 26.9 %all-to-all-start.1 = ((bf16[16,16,1536]{2,1,0:T(8,128)(2,1)}), bf16[16,16,1536]{2,1,0:T(8,128)(2,1)S(1)}, u32[]{:S(2)}, u32[]{:S(2)}) async-start(bf16[16,16,1536]{2,1,0:T(8,128)(2,1)} %reduce-scatter.2.cloned.1.call-done), calls=%async_computation.2 | async-start | bytes 1572864 | tf_op jit(solution)/shard_map/all_to_all | solution.py:117
Sparse Core Ops, SparseCore 0:
  19.7 20.7 all-reduce.1
  110.1 7.2 reduce-scatter.1
where the time goes:
time: 153 us; the launch traced here: 152 us
  waiting for transfers between devices  45.9 us (30%)
  blocking collectives  44.6 us (29%)
  matrix products  33.3 us (22%)
  between operations  14.3 us (9%)
  starting transfers between devices  6.98 us (5%)
  other arithmetic  4.03 us (3%)
  local copies, waits for them, and re-layouts  3.47 us (2%)
    all_to_all x1, blocking collectives, per_device(): lax.all_to_all(outgoing, 'ep', split_axis=0, concat_axis=0, tiled=True)  44.6 us
    psum x1, waiting for transfers between devices, per_device(): lax.psum(partial_value.astype(jnp.float32).astype(jnp.bfloat16), 'tp')  20 us
    all_to_all x1, waiting for transfers between devices, per_device(): lax.all_to_all(halves.astype(jnp.bfloat16), 'ep', split_axis=0, concat_ax...  18.4 us
    dot_general x1, matrix products, per_device(): produced = jnp.dot(hidden, w_down, preferred_element_type=jnp.float32)  16.3 us
    reduce_scatter x1, waiting for transfers between devices, per_device(): lax.psum_scatter(produced.astype(jnp.bfloat16), 'tp', scatter_dimension=2...  7.46 us
    all_to_all x1, starting transfers between devices, per_device(): lax.all_to_all(halves.astype(jnp.bfloat16), 'ep', split_axis=0, concat_ax...  6.9 us
    dot_general x1, matrix products, per_device(): gated = jnp.dot(rows, w_gate, preferred_element_type=jnp.float32)  6.77 us
    dot_general x1, matrix products, per_device(): jnp.dot(activated, w_out, preferred_element_type=jnp.float32)  3.96 us
  transfers between devices with their start and end apart: 3, of which 3 were waited for; matrix products, arithmetic and copies ran while one was open for 2% of the time, Pallas kernels for 0%

commit v1 on v0

--- a/solution.py
+++ b/solution.py
@@ -81,9 +81,9 @@
     partial_value = jnp.dot(activated, w_out, preferred_element_type=jnp.float32).astype(
         jnp.bfloat16
     )
-    summed = lax.psum(partial_value.astype(jnp.float32).astype(jnp.bfloat16), "tp").astype(
-        jnp.float32
-    )
+    summed = jnp.sum(
+        lax.all_gather(partial_value.astype(jnp.float32).astype(jnp.bfloat16), "tp"), axis=0
+    ).astype(jnp.float32)
     mixed = (tokens.astype(jnp.float32) + summed).astype(jnp.bfloat16)
     expert_in = normalize(mixed, expert_gain)
     weights = route_weights(route_logit)

time: 153 us -> 137 us (0.90)
  waiting for transfers between devices: 45.9 us -> 25.8 us
  blocking collectives: 44.6 us -> 48.2 us
    psum x1 -> x0, waiting for transfers between devices: 20 us -> none  [per_device(): lax.psum(partial_value.astype(jnp.float32).astype(jnp.bfloat16), 'tp')]
    all_gather x0 -> x1, blocking collectives: none -> 2.35 us  [per_device(): lax.all_gather(partial_value.astype(jnp.float32).astype(jnp.bfloat16), 'tp')]
  transfers between devices with their start and end apart: 3 -> 2, of which waited for: 3 -> 2; matrix products, arithmetic and copies ran while one was open for 2% -> 1% of each run, Pallas kernels for 0% -> 0%
where the time goes in v1:
time: 137 us
  blocking collectives  48.2 us (35%)
  matrix products  32.6 us (24%)
  waiting for transfers between devices  25.8 us (19%)
  between operations  14.2 us (10%)
  starting transfers between devices  6.95 us (5%)
  other arithmetic  4.67 us (3%)
  local copies, waits for them, and re-layouts  4.13 us (3%)
    all_to_all x1, blocking collectives, per_device(): lax.all_to_all(outgoing, 'ep', split_axis=0, concat_axis=0, tiled=True)  45.9 us
    all_to_all x1, waiting for transfers between devices, per_device(): lax.all_to_all(halves.astype(jnp.bfloat16), 'ep', split_axis=0, concat_ax...  18.4 us
    dot_general x1, matrix products, per_device(): produced = jnp.dot(hidden, w_down, preferred_element_type=jnp.float32)  16.3 us
    reduce_scatter x1, waiting for transfers between devices, per_device(): lax.psum_scatter(produced.astype(jnp.bfloat16), 'tp', scatter_dimension=2...  7.43 us
    all_to_all x1, starting transfers between devices, per_device(): lax.all_to_all(halves.astype(jnp.bfloat16), 'ep', split_axis=0, concat_ax...  6.91 us
    dot_general x1, matrix products, per_device(): gated = jnp.dot(rows, w_gate, preferred_element_type=jnp.float32)  6.77 us
    dot_general x1, matrix products, per_device(): jnp.dot(normed, w_in, preferred_element_type=jnp.float32)  3.47 us
    dot_general x1, matrix products, per_device(): jnp.dot(activated, w_out, preferred_element_type=jnp.float32)  3.26 us
  transfers between devices with their start and end apart: 2, of which 2 were waited for; matrix products, arithmetic and copies ran while one was open for 1% of the time, Pallas kernels for 0%

profile of v1, /device:TPU:0, one launch (start us, length us, event | category | flops | bytes accessed | tf_op | source)
XLA Modules:
  0.0 136.6 jit_solution(17342804729848064801)
XLA Ops:
  7.2 0.7 exp.18
  7.9 1.1 fusion.9
  9.0 0.8 add_divide_fusion.1
  9.8 0.8 copy.50
  11.2 0.7 multiply_add_fusion.1
  11.9 3.5 %convolution_convert_fusion.3 = bf16[32,768]{1,0:T(8,128)(2,1)S(1)} fusion(bf16[3072,768]{1,0:T(8,128)(2,1)} %param.26, bf16[32,3072]{1,0:T(8,128)(2,1)} %param.17, f32[3072]{0:T(1024)} %param.25, f32[32]{0:T(128)S(1)} %add_rsqrt_fusion.1), kind=kOutput, calls=%fused_computation.9 | convolution fusion | flops 151412736 | bytes 4976768 | tf_op jit(solution)/shard_map/dot_general | solution.py:77
  15.6 0.3 fusion.44
  15.9 0.3 convolution_bitcast_fusion
  16.3 0.2 cosine_multiply_fusion
  16.5 0.8 fusion.43
  17.4 0.8 fusion.2
  18.4 3.3 %convolution_convert_fusion.2 = bf16[32,3072]{1,0:T(8,128)(2,1)S(1)} fusion(bf16[768,3072]{1,0:T(8,128)(2,1)} %param.27, f32[32,768]{1,0:T(8,128)S(1)} %copy.49, bf16[32,768]{1,0:T(8,128)(2,1)S(1)} %convolution_convert_fusion.3, f32[768]{0:T(1024)S(1)} %copy-done.7), kind=kOutput, calls=%fused_computation.2 | convolution fusion | flops 151388160 | bytes 5065728 | tf_op jit(solution)/shard_map/dot_general | solution.py:81
  21.7 2.3 %all-gather = bf16[64,3072]{1,0:T(8,128)(2,1)S(1)} all-gather(bf16[32,3072]{1,0:T(8,128)(2,1)S(1)} %convolution_convert_fusion.2), channel_id=2, replica_groups=mesh['ep'=16,'tp'=2] {'tp'}, dimensions={0}, use_global_device_ids=true | all-gather | bytes 589824 | tf_op jit(solution)/shard_map/all_gather | solution.py:85
  24.5 0.4 convolution_convert_fusion.1
  24.9 0.2 broadcast_in_dim.2
  25.1 45.9 %all_to_all.10 = bf16[16,16,3072]{2,1,0:T(8,128)(2,1)S(1)} all-to-all(bf16[16,16,3072]{2,1,0:T(8,128)(2,1)S(1)} %bitcast.28), channel_id=1, replica_groups=mesh['ep'=16,'tp'=2] {'ep'}, dimensions={0} | all-to-all | bytes 3145728 | tf_op jit(solution)/shard_map/all_to_all | solution.py:106
  71.0 6.8 %fusion.45 = f32[256,1344]{0,1:T(8,128)} fusion(bf16[256,3072]{1,0:T(8,128)(2,1)S(1)} %bitcast.32, bf16[3072,1344]{0,1:T(8,128)(2,1)} %param.31), kind=kOutput, calls=%fused_computation.74 | convolution fusion | flops 2113929216 | bytes 11206656 | tf_op jit(solution)/shard_map/dot_general | solution.py:109
  77.7 16.3 %convolution_convert_fusion = bf16[256,3072]{1,0:T(8,128)(2,1)} fusion(bf16[1344,3072]{1,0:T(8,128)(2,1)} %param.33, bf16[256,3072]{1,0:T(8,128)(2,1)S(1)} %bitcast.33, bf16[3072,1344]{0,1:T(8,128)(2,1)} %param.32, f32[256,1344]{0,1:T(8,128)} %fusion.45), kind=kOutput, calls=%fused_computation | convolution fusion | flops 4230709248 | bytes 21037056 | tf_op jit(solution)/shard_map/dot_general | solution.py:112
  94.1 7.4 %reduce-scatter.2.cloned.1.call-done = bf16[16,16,1536]{2,1,0:T(8,128)(2,1)} async-done(((bf16[16,16,3072]{2,1,0:T(8,128)(2,1)}), bf16[16,16,1536]{2,1,0:T(8,128)(2,1)}) %reduce-scatter.2.cloned.1.call-update) | async-done | bytes 786448 | tf_op jit(solution)/shard_map/reduce_scatter | solution.py:114
  101.5 6.9 %all-to-all-start.1 = ((bf16[16,16,1536]{2,1,0:T(8,128)(2,1)}), bf16[16,16,1536]{2,1,0:T(8,128)(2,1)S(1)}, u32[]{:S(2)}, u32[]{:S(2)}) async-start(bf16[16,16,1536]{2,1,0:T(8,128)(2,1)} %reduce-scatter.2.cloned.1.call-done), calls=%async_computation.2 | async-start | bytes 1572864 | tf_op jit(solution)/shard_map/all_to_all | solution.py:117
  108.4 0.3 pad_maximum_fusion
  108.7 1.3 copy.52
  110.1 18.4 %all-to-all-done.1 = bf16[16,16,1536]{2,1,0:T(8,128)(2,1)S(1)} async-done(((bf16[16,16,1536]{2,1,0:T(8,128)(2,1)}), bf16[16,16,1536]{2,1,0:T(8,128)(2,1)S(1)}, u32[]{:S(2)}, u32[]{:S(2)}) %all-to-all-start.1) | async-done | bytes 786464 | tf_op jit(solution)/shard_map/all_to_all | solution.py:117
  128.6 1.2 fusion.1
  (33 shorter events, 1.8 us)
Async XLA Ops:
  7.2 8.7 %copy-start = (bf16[48,128,16]{1,2,0:T(8,128)(2,1)S(1)}, bf16[48,128,16]{1,2,0:T(8,128)(2,1)}, u32[]{:S(2)}) copy-start(bf16[48,128,16]{1,2,0:T(8,128)(2,1)} %param.22) | copy-start | bytes 589828
  7.2 94.3 %reduce-scatter.2.cloned.1.call-start = ((), (), s32[]{:S(2)}) async-start(), calls=%async_computation.3 | async-start | bytes 2359296 | tf_op jit(solution)/shard_map/reduce_scatter | solution.py:114
  11.9 3.7 %copy-start.1 = (f32[32,48,128]{2,1,0:T(8,128)S(1)}, f32[32,48,128]{2,1,0:T(8,128)}, u32[]{:S(2)}) copy-start(f32[32,48,128]{2,1,0:T(8,128)} %param.18) | copy-start | bytes 2359300
  15.6 0.7 copy-start.4
  15.6 0.7 copy-start.5
  16.5 0.9 copy-start.3
  17.3 1.1 copy-start.7
  18.4 5.7 %copy-start.2 = (bf16[32,3072]{1,0:T(8,128)(2,1)S(1)}, bf16[32,3072]{1,0:T(8,128)(2,1)}, u32[]{:S(2)}) copy-start(bf16[32,3072]{1,0:T(8,128)(2,1)} %param.17) | copy-start | bytes 589828
  21.7 2.8 %copy-start.6 = (f32[3072]{0:T(1024)S(1)}, f32[3072]{0:T(1024)}, u32[]{:S(2)}) copy-start(f32[3072]{0:T(1024)} %param.28) | copy-start | bytes 36868
  101.5 26.9 %all-to-all-start.1 = ((bf16[16,16,1536]{2,1,0:T(8,128)(2,1)}), bf16[16,16,1536]{2,1,0:T(8,128)(2,1)S(1)}, u32[]{:S(2)}, u32[]{:S(2)}) async-start(bf16[16,16,1536]{2,1,0:T(8,128)(2,1)} %reduce-scatter.2.cloned.1.call-done), calls=%async_computation.2 | async-start | bytes 1572864 | tf_op jit(solution)/shard_map/all_to_all | solution.py:117
Sparse Core Ops, SparseCore 0:
  94.2 7.2 reduce-scatter.1
